TPU v7x, 32 devices: a whole 2x2x4 slice. The times are simulated.
32 devices in a mesh: grp: 2 (over y), fs: 4 (over z), tp: 4 (over x, core).
Axes of the slice: x: 2, y: 2, z: 4, core: 2. Of those that a mesh axis runs over, the one named last changes fastest.
Arguments:
- prompt: bfloat16 [8, 1024, 2048], P(('grp', 'tp')), parts along dimension 0, may hold values from -6 to 6
- gate_first: float32 [2048, 5632], P('fs', 'tp'), may hold values from -0.125 to 0.125
- up_first: float32 [2048, 5632], P('fs', 'tp'), may hold values from -0.125 to 0.125
- down_first: float32 [5632, 2048], P('fs', 'tp'), may hold values from -0.3125 to 0.3125
- norm_gain: float32 [2048], replicated, may hold values from 0.1 to 1.9
- gate_second: float32 [2048, 5632], P('fs', 'tp'), may hold values from -0.125 to 0.125
- up_second: float32 [2048, 5632], P('fs', 'tp'), may hold values from -0.125 to 0.125
- down_second: float32 [5632, 2048], P('fs', 'tp'), may hold values from -0.3125 to 0.3125
Outputs:
- result: bfloat16 [8, 1024, 2048], P(('grp', 'tp'), 'fs'), parts along dimension 0
- gate_one: bfloat16 [4096, 5632], P('grp', 'fs'), parts along dimension 0
- up_one: bfloat16 [4096, 5632], P('grp', 'fs'), parts along dimension 0
- down_one: bfloat16 [5632, 4096], P('fs', 'grp'), parts along dimension 1
- gate_two: bfloat16 [4096, 5632], P('grp', 'fs'), parts along dimension 0
- up_two: bfloat16 [4096, 5632], P('grp', 'fs'), parts along dimension 0
- down_two: bfloat16 [5632, 4096], P('fs', 'grp'), parts along dimension 1
There are 2 independent parts, one for each index of `grp`. A program takes and returns all parts, laid end to end along the dimension named above; an argument that names none is the same for every part. Nothing has to cross between parts.
All inputs are finite; a program needn't handle non-finite values.
Results may differ from a plain program's by a relative error of at most 0.029.
Values may be sent and summed in bfloat16 or wider, within the bound.
A program may use at most 192 MiB of HBM per device.

v0:
```python
import jax
import jax.numpy as jnp
from jax import lax
from jax.experimental import pallas as pl
from jax.experimental.pallas import tpu as pltpu
from jax.sharding import PartitionSpec as P

norm_eps = 1e-05
deep_alpha = 2.0**0.25
half_step = 0.5
lane = 128
steps = 8
MESH = pl.DeviceIdType.MESH
ANY = pl.BlockSpec(memory_space=pl.ANY)
VMEM = pl.BlockSpec(memory_space=pltpu.VMEM)


def plain_norm(values):
    row_mean = jnp.mean(values, axis=-1, keepdims=True)
    centred = values - row_mean
    variance = jnp.mean(centred * centred, axis=-1, keepdims=True)
    return centred * lax.rsqrt(variance + norm_eps)


def gated_hidden(inputs, gate_proj, up_proj):
    gate_act = jnp.dot(inputs, gate_proj, preferred_element_type=jnp.float32)
    up_act = jnp.dot(inputs, up_proj, preferred_element_type=jnp.float32)
    return (jax.nn.silu(gate_act) * up_act).astype(jnp.bfloat16)


def relay_weights(gate_proj, up_proj, down_proj):
    gate_rows, up_rows, down_mine = (
        lax.all_gather(gate_proj, "tp", axis=1, tiled=True),
        lax.all_gather(up_proj, "tp", axis=1, tiled=True),
        lax.all_gather(down_proj, "tp", axis=1, tiled=True),
    )
    gate_mine, up_mine = (
        lax.all_to_all(gate_rows, "fs", split_axis=1, concat_axis=0, tiled=True),
        lax.all_to_all(up_rows, "fs", split_axis=1, concat_axis=0, tiled=True),
    )
    return (gate_mine, up_mine, down_mine)


def general_blocks(tokens, norm_gain, first, second):
    fs_index, fs_count = lax.axis_index("fs"), lax.axis_size("fs")
    own_count = tokens.shape[0] // fs_count

    def summed(rows, projs):
        terms = jnp.dot(
            gated_hidden(rows, projs[0], projs[1]), projs[2], preferred_element_type=jnp.float32
        ).astype(jnp.bfloat16)
        parts = lax.all_to_all(
            terms.reshape(fs_count, own_count, -1), "fs", split_axis=0, concat_axis=0
        )
        return jnp.sum(parts.astype(jnp.float32), axis=0)

    own_tokens = lax.dynamic_slice_in_dim(tokens, fs_index * own_count, own_count, 0)
    first = relay_weights(*first)
    second = relay_weights(*second)
    normed_own = plain_norm(
        deep_alpha * own_tokens.astype(jnp.float32) + half_step * summed(tokens, first)
    ).astype(jnp.bfloat16)
    normed = lax.all_gather(normed_own, "fs", axis=0, tiled=True)
    ffn_two = summed(normed, second)
    residual_two = deep_alpha * norm_gain * normed_own.astype(jnp.float32)
    return (plain_norm(residual_two + half_step * ffn_two).astype(jnp.bfloat16), *first, *second)


class Here:
    def __init__(self):
        self.g, self.f, self.t = (lax.axis_index(name) for name in ("grp", "fs", "tp"))
        side = lax.axis_size("tp")
        self.side = side
        self.x, self.c = self.t // 2, self.t % 2
        self.q = self.g * 2 + self.x
        self.xt = (self.t + 2) % side
        self.ct = self.t + 1 - 2 * self.c
        self.xn = (self.g, self.f, self.xt)
        self.yn = (1 - self.g, self.f, self.t)
        self.cn = (self.g, self.f, self.ct)
        last = lax.axis_size("fs") - 1
        self.m = self.f // 2
        self.end = self.f + self.m * (last - 2 * self.f)
        self.inner = (self.g, self.f + 1 - 2 * self.m, self.t)
        self.outer = (self.g, self.f - 1 + 2 * self.m, self.t)
        self.last = last

    def owner(self, mirrored):
        return mirrored + self.m * (self.last - 2 * mirrored)

    def order(self, k):
        f = self.f
        return (f, f + 1 - 2 * (f % 2), (f + 2) % self.side, self.last - f)[k]


def remote(src, dst, send_sem, recv_sem, device):
    return pltpu.make_async_remote_copy(
        src_ref=src,
        dst_ref=dst,
        send_sem=send_sem,
        recv_sem=recv_sem,
        device_id=device,
        device_id_type=MESH,
    )


class PlaneGather:
    kinds = 9

    def __init__(self, here, w, sems):
        self.h, self.w, self.sems = here, w, sems
        self.rows = w.shape[1] // here.side
        self.piece = self.rows // 4
        self.cut = self.piece * 3 // 4
        self.started = []

    def region(self, which, z, q, first, count):
        return self.w.at[which, pl.ds(z * self.rows + q * self.piece + first, count)]

    def send(self, z, kind, region, device):
        copy = remote(region, region, self.sems.at[0, z, kind], self.sems.at[1, z, kind], device)
        copy.start()
        self.started.append(copy)

    def arrive(self, z, kind, region):
        remote(
            region, region, self.sems.at[0, z, kind], self.sems.at[1, z, kind], self.h.cn
        ).wait_recv()

    def own(self, k):
        h, z = self.h, self.h.order(k)
        region = self.region(h.c, z, h.q, 0, self.piece)
        self.send(z, 0, region, h.xn)
        self.send(z, 1, region, h.yn)
        self.send(z, 4, region, h.cn)

    def quarters(self):
        h = self.h
        return (h.g * 2 + 1 - h.x, (1 - h.g) * 2 + h.x, (1 - h.g) * 2 + 1 - h.x)

    def forward(self, k):
        h, z = self.h, self.h.order(k)
        from_x, from_y, unused = self.quarters()
        region = self.region(h.c, z, from_x, 0, self.piece)
        self.arrive(z, 0, region)
        self.send(z, 2, self.region(h.c, z, from_x, 0, self.cut), h.yn)
        self.send(z, 5, region, h.cn)
        region = self.region(h.c, z, from_y, 0, self.piece)
        self.arrive(z, 1, region)
        self.send(z, 3, self.region(h.c, z, from_y, self.cut, self.piece - self.cut), h.xn)
        self.send(z, 6, region, h.cn)

    def corner(self, k):
        h, z = self.h, self.h.order(k)
        across = self.quarters()[2]
        region = self.region(h.c, z, across, 0, self.cut)
        self.arrive(z, 2, region)
        self.send(z, 7, region, h.cn)
        region = self.region(h.c, z, across, self.cut, self.piece - self.cut)
        self.arrive(z, 3, region)
        self.send(z, 8, region, h.cn)

    def finish(self):
        h, other = self.h, 1 - self.h.c
        from_x, from_y, across = self.quarters()
        for k in range(h.side):
            z = h.order(k)
            self.arrive(z, 4, self.region(other, z, h.q, 0, self.piece))
            self.arrive(z, 5, self.region(other, z, from_x, 0, self.piece))
            self.arrive(z, 6, self.region(other, z, from_y, 0, self.piece))
            self.arrive(z, 7, self.region(other, z, across, 0, self.cut))
            self.arrive(z, 8, self.region(other, z, across, self.cut, self.piece - self.cut))
        for copy in self.started:
            copy.wait_send()


class DownGather:
    kinds = 5

    def __init__(self, here, src, dst, sems, bounce, local):
        self.h, self.src, self.dst, self.sems = here, src, dst, sems
        self.bounce, self.local = bounce, local
        self.rows, self.cols = src.shape
        self.half = self.rows // 2
        self.started = []

    def columns(self, t):
        return pl.ds(pl.multiple_of(t * self.cols, self.cols), self.cols)

    def part(self, g, t):
        return self.dst.at[pl.ds(g * self.half, self.half), self.columns(t)]

    def send(self, kind, src, dst, device):
        copy = remote(src, dst, self.sems.at[0, kind], self.sems.at[1, kind], device)
        copy.start()
        self.started.append(copy)

    def arrive(self, kind, region):
        remote(
            region, region, self.sems.at[0, kind], self.sems.at[1, kind], self.h.cn
        ).wait_recv()

    def begin(self):
        h = self.h
        self.take = pltpu.make_async_copy(self.src, self.bounce, self.local.at[0])
        self.take.start()
        self.send(
            0, self.src.at[pl.ds(h.g * self.half, self.half)], self.part(h.g, h.t), h.xn
        )
        self.send(2, self.src, self.dst.at[:, self.columns(h.t)], h.cn)

    def place(self):
        self.take.wait()
        self.put = pltpu.make_async_copy(
            self.bounce, self.dst.at[:, self.columns(self.h.t)], self.local.at[1]
        )
        self.put.start()

    def forward(self):
        h = self.h
        region = self.part(h.g, h.xt)
        self.arrive(0, region)
        self.send(1, region, region, h.yn)
        self.send(3, region, region, h.cn)

    def corner(self):
        h = self.h
        region = self.part(1 - h.g, h.xt)
        self.arrive(1, region)
        self.send(4, region, region, h.cn)

    def finish(self):
        h = self.h
        across = (h.ct + 2) % h.side
        self.arrive(2, self.dst.at[:, self.columns(h.ct)])
        self.arrive(3, self.part(h.g, across))
        self.arrive(4, self.part(1 - h.g, across))
        self.put.wait()
        for copy in self.started:
            copy.wait_send()


class Placement:
    def __init__(self, here, src, dst, send_sem, recv_sem, bounce, local):
        self.h, self.src, self.dst = here, src, dst
        self.send_sem, self.recv_sem, self.bounce, self.local = send_sem, recv_sem, bounce, local
        self.rows = src.shape[1]
        self.piece = self.rows // 4

    def copies(self):
        h = self.h
        for x in range(2):
            for c in range(2):
                target, q = 2 * x + c, h.g * 2 + x
                mine = jnp.logical_and(h.f == h.t, h.t == target)
                src = self.src.at[c, pl.ds(q * self.piece, self.piece)]
                dst = self.dst.at[c, pl.ds(h.f * self.rows + q * self.piece, self.piece)]
                copy = remote(
                    src, dst, self.send_sem.at[target], self.recv_sem.at[h.f], (h.g, h.t, target)
                )
                yield mine, src, dst, copy

    def begin(self):
        for mine, src, dst, copy in self.copies():

            @pl.when(jnp.logical_not(mine))
            def _():
                copy.start()

            @pl.when(mine)
            def _():
                take = pltpu.make_async_copy(src, self.bounce, self.local)
                take.start()
                take.wait()
                put = pltpu.make_async_copy(self.bounce, dst, self.local)
                put.start()
                put.wait()

    def arrived(self, k):
        h = self.h
        z = h.order(k)
        region = self.dst.at[h.c, pl.ds(z * self.rows + h.q * self.piece, self.piece)]
        copy = remote(region, region, self.send_sem.at[0], self.recv_sem.at[z], h.cn)
        if k == 0:

            @pl.when(h.f != h.t)
            def _():
                copy.wait_recv()

        else:
            copy.wait_recv()

    def finish(self):
        for mine, src, dst, copy in self.copies():

            @pl.when(jnp.logical_not(mine))
            def _():
                copy.wait_send()


def weights_kernel(
    src_one, down_src, src_two, w_one, down_one, w_two,
    bounce, down_bounce, place_sems, plane_sems, down_sems, local,
):
    h = Here()
    first = Placement(
        h, src_one, w_one, place_sems.at[0, 0], place_sems.at[0, 1], bounce, local.at[2]
    )
    second = Placement(
        h, src_two, w_two, place_sems.at[1, 0], place_sems.at[1, 1], bounce, local.at[2]
    )
    gather = PlaneGather(h, w_one, plane_sems)
    down = DownGather(h, down_src, down_one, down_sems, down_bounce, local)
    first.begin()
    down.begin()
    down.place()
    for k in range(h.side):
        first.arrived(k)
        gather.own(k)
        if k == 1:
            down.forward()
        if k >= 1:
            gather.forward(k - 1)
        if k >= 2:
            gather.corner(k - 2)
        if k == 2:
            second.begin()
            down.corner()
    gather.forward(h.side - 1)
    gather.corner(h.side - 2)
    gather.corner(h.side - 1)
    gather.finish()
    down.finish()
    for k in range(h.side):
        second.arrived(k)
    first.finish()
    second.finish()


def gather_weights(src_one, down_src, src_two):
    side = lax.axis_size("tp")
    two, rows, width = src_one.shape
    full = jax.ShapeDtypeStruct((two, rows * side, width), src_one.dtype)
    down = jax.ShapeDtypeStruct((down_src.shape[0], down_src.shape[1] * side), down_src.dtype)
    return pl.pallas_call(
        weights_kernel,
        out_shape=(full, down, full),
        in_specs=[ANY] * 3,
        out_specs=(ANY,) * 3,
        scratch_shapes=[
            pltpu.VMEM((rows // 4, width), src_one.dtype),
            pltpu.VMEM(down_src.shape, down_src.dtype),
            pltpu.SemaphoreType.DMA((2, 2, side)),
            pltpu.SemaphoreType.DMA((2, side, PlaneGather.kinds)),
            pltpu.SemaphoreType.DMA((2, DownGather.kinds)),
            pltpu.SemaphoreType.DMA((3,)),
        ],
        compiler_params=pltpu.CompilerParams(has_side_effects=True),
        name="gather_weights",
    )(src_one, down_src, src_two)


def compute_kernel(
    tokens, w, down, terms, gate_out, up_out, down_out,
    rows_in, w_in, down_in, hidden, terms_in, sems,
):
    groups = w.shape[2] // lane
    wide = 2 * lane
    spans = down.shape[1] // wide
    count = tokens.shape[0]
    block = count // 4

    def w_load(which, j):
        return pltpu.make_async_copy(
            w.at[which, :, pl.ds(pl.multiple_of(j * lane, lane), lane)],
            w_in.at[j, :, pl.ds(which * lane, lane)],
            sems.at[which, j],
        )

    def w_store(which, j):
        return pltpu.make_async_copy(
            w_in.at[j, :, pl.ds(which * lane, lane)],
            (gate_out, up_out)[which].at[:, pl.ds(pl.multiple_of(j * lane, lane), lane)],
            sems.at[2 + which, j],
        )

    take_rows = pltpu.make_async_copy(tokens, rows_in, sems.at[4, 0])
    take_down = pltpu.make_async_copy(down, down_in, sems.at[4, 1])
    give_down = pltpu.make_async_copy(down_in, down_out, sems.at[4, 2])
    take_rows.start()

    @pl.loop(0, groups)
    def _(j):
        w_load(0, j).start()
        w_load(1, j).start()

    take_down.start()
    take_rows.wait()

    @pl.loop(0, groups)
    def _(j):
        w_load(0, j).wait()
        w_load(1, j).wait()
        w_store(0, j).start()
        w_store(1, j).start()

        @pl.loop(0, 4)
        def _(r):
            at = pl.ds(pl.multiple_of(r * block, block), block)
            act = jnp.dot(rows_in[at, :], w_in[j], preferred_element_type=jnp.float32)
            gate_act, up_act = act[:, :lane], act[:, lane:]
            value = gate_act / (1.0 + jnp.exp(-gate_act)) * up_act
            hidden[at, pl.ds(pl.multiple_of(j * lane, lane), lane)] = value.astype(jnp.bfloat16)

    take_down.wait()
    give_down.start()

    @pl.loop(0, spans)
    def _(n):
        cols = pl.ds(pl.multiple_of(n * wide, wide), wide)

        @pl.loop(0, 4)
        def _(r):
            at = pl.ds(pl.multiple_of(r * block, block), block)
            terms_in[at, cols] = jnp.dot(
                hidden[at, :], down_in[:, cols], preferred_element_type=jnp.float32
            ).astype(jnp.bfloat16)

    give_terms = pltpu.make_async_copy(terms_in, terms, sems.at[4, 3])
    give_terms.start()

    @pl.loop(0, groups)
    def _(j):
        w_store(0, j).wait()
        w_store(1, j).wait()

    give_down.wait()
    give_terms.wait()


def compute_terms(tokens, w, down):
    two, depth, width = w.shape
    count = tokens.shape[0]
    groups = width // lane
    proj = jax.ShapeDtypeStruct((depth, width), w.dtype)
    flops = 2 * count * depth * width * 3
    return pl.pallas_call(
        compute_kernel,
        out_shape=(
            jax.ShapeDtypeStruct((count, down.shape[1]), jnp.bfloat16),
            proj,
            proj,
            jax.ShapeDtypeStruct(down.shape, down.dtype),
        ),
        in_specs=[ANY] * 3,
        out_specs=(ANY,) * 4,
        scratch_shapes=[
            pltpu.VMEM(tokens.shape, tokens.dtype),
            pltpu.VMEM((groups, depth, 2 * lane), w.dtype),
            pltpu.VMEM(down.shape, down.dtype),
            pltpu.VMEM((count, width), jnp.bfloat16),
            pltpu.VMEM((count, down.shape[1]), jnp.bfloat16),
            pltpu.SemaphoreType.DMA((5, max(groups, 4))),
        ],
        compiler_params=pltpu.CompilerParams(vmem_limit_bytes=56 * 1024 * 1024),
        cost_estimate=pl.CostEstimate(flops=flops, bytes_accessed=6 * w.size, transcendentals=0),
        name="compute_terms",
    )(tokens, w, down)


class LineSum:
    kinds = 6

    def __init__(self, here, terms, from_outer, from_inner, from_middle, to_inner, to_outer, sems):
        self.h, self.terms = here, terms
        self.from_outer, self.from_inner, self.from_middle = from_outer, from_inner, from_middle
        self.to_inner, self.to_outer, self.sems = to_inner, to_outer, sems
        self.own = terms.shape[0] // (here.last + 1)
        self.size = self.own // steps

    def term(self, mirrored, s):
        first = self.h.owner(mirrored) * self.own + s * self.size
        return pl.ds(pl.multiple_of(first, self.size), self.size)

    def at(self, s):
        return pl.ds(pl.multiple_of(s * self.size, self.size), self.size)

    def copy(self, src, dst, kind, s, device):
        return remote(src, dst, self.sems.at[0, kind, s], self.sems.at[1, kind, s], device)

    def start_copy(self, o, s):
        slot = 3 - o
        return self.copy(
            self.terms.at[self.term(o, s)], self.from_outer.at[slot, self.at(s)], slot, s,
            self.h.inner,
        )

    def middle_copy(self, o, s):
        slot = 3 - o
        return self.copy(
            self.to_inner.at[slot, self.at(s)], self.from_middle.at[slot, self.at(s)], 3 + slot,
            s, self.h.inner,
        )

    def back_copy(self, s):
        return self.copy(
            self.to_outer.at[self.at(s)], self.from_inner.at[self.at(s)], 5, s, self.h.outer
        )

    def send_start(self, s):
        for o in (3, 2, 1):
            self.start_copy(o, s).start()

    def relay(self, s):
        at = self.at(s)
        for o in (3, 2):
            slot = 3 - o
            self.start_copy(o, s).wait_recv()
            self.to_inner[slot, at, :] = (
                self.from_outer[slot, at, :].astype(jnp.float32)
                + self.terms[self.term(o, s), :].astype(jnp.float32)
            ).astype(jnp.bfloat16)
            self.middle_copy(o, s).start()

    def relay_back(self, s):
        at = self.at(s)
        self.middle_copy(3, s).wait_recv()
        self.to_outer[at, :] = (
            self.from_middle[0, at, :].astype(jnp.float32)
            + self.terms[self.term(0, s), :].astype(jnp.float32)
        ).astype(jnp.bfloat16)
        self.back_copy(s).start()

    def inner_total(self, s):
        at = self.at(s)
        self.start_copy(1, s).wait_recv()
        self.middle_copy(2, s).wait_recv()
        return (
            self.from_outer[2, at, :].astype(jnp.float32)
            + self.terms[self.term(1, s), :].astype(jnp.float32)
        ) + self.from_middle[1, at, :].astype(jnp.float32)

    def end_total(self, s):
        at = self.at(s)
        self.back_copy(s).wait_recv()
        return self.terms[self.term(0, s), :].astype(jnp.float32) + self.from_inner[
            at, :
        ].astype(jnp.float32)

    def finish_end(self, s):
        for o in (3, 2, 1):
            self.start_copy(o, s).wait_send()

    def finish_inner(self, s):
        self.middle_copy(3, s).wait_send()
        self.middle_copy(2, s).wait_send()
        self.back_copy(s).wait_send()


def line_scratch(own, width):
    def rows(*lead):
        return pltpu.VMEM((*lead, own, width), jnp.bfloat16)

    return [
        rows(3), rows(), rows(2), rows(2), rows(),
        pltpu.SemaphoreType.DMA((2, LineSum.kinds, steps)),
    ]


class LineSpread:
    kinds = 6

    def __init__(self, here, out, sems, own):
        self.h, self.out, self.sems, self.own = here, out, sems, own
        self.size = own // steps

    def rows(self, mirrored, s):
        first = self.h.owner(mirrored) * self.own + s * self.size
        return self.out.at[pl.ds(pl.multiple_of(first, self.size), self.size)]

    def copy(self, mirrored, kind, s, device, src=None):
        rows = self.rows(mirrored, s)
        return remote(
            rows if src is None else src, rows, self.sems.at[0, kind, s], self.sems.at[1, kind, s],
            device,
        )

    def in_zero(self, s, src=None):
        return self.copy(0, 0, s, self.h.inner, src)

    def cross_one(self, s, src=None):
        return self.copy(1, 1, s, self.h.inner, src)

    def cross_zero(self, s):
        return self.copy(0, 2, s, self.h.inner)

    def out_any(self, o, s, src=None):
        return self.copy(o, 2 + o, s, self.h.outer, src)


def middle_kernel(
    terms, tokens, w_in, down_src, gathered, w, down,
    own_rows, normed, down_bounce,
    from_outer, from_inner, from_middle, to_inner, to_outer, line_sems,
    spread_sems, plane_sems, down_sems, local,
):
    h = Here()
    own = normed.shape[0]
    size = own // steps
    is_end = h.end == 0
    is_inner = h.end == 1
    line = LineSum(h, terms, from_outer, from_inner, from_middle, to_inner, to_outer, line_sems)
    spread = LineSpread(h, gathered, spread_sems, own)
    gather = PlaneGather(h, w, plane_sems)
    down_part = DownGather(h, down_src, down, down_sems, down_bounce, local)
    take = pltpu.make_async_copy(
        tokens.at[pl.ds(pl.multiple_of(h.f * own, own), own)], own_rows, local.at[2]
    )
    take.start()

    @pl.when(is_end)
    def _():
        line.send_start(0)
        line.send_start(1)

    down_part.begin()
    for k in range(h.side):
        gather.own(k)
    down_part.place()
    take.wait()

    def keep(s, total):
        at = pl.ds(s * size, size)
        normed[at, :] = plain_norm(
            deep_alpha * own_rows[at, :].astype(jnp.float32) + half_step * total
        ).astype(jnp.bfloat16)
        return normed.at[at]

    def put_own(s):
        first = h.f * own + s * size
        return pltpu.make_async_copy(
            normed.at[pl.ds(s * size, size)],
            gathered.at[pl.ds(pl.multiple_of(first, size), size)],
            local.at[3 + s],
        )

    def hand_on(s):
        @pl.when(is_inner)
        def _():
            spread.in_zero(s).wait_recv()
            spread.cross_zero(s).start()
            spread.cross_one_in(s).wait_recv()
            spread.out_any(2, s).start()
            spread.cross_zero_in(s).wait_recv()
            spread.out_any(3, s).start()

    spread.cross_one_in = lambda s: spread.copy(2, 1, s, h.inner)
    spread.cross_zero_in = lambda s: spread.copy(3, 2, s, h.inner)

    jobs = {
        1: [lambda: gather.forward(0), down_part.forward],
        2: [lambda: gather.forward(1)],
        3: [lambda: gather.forward(2), down_part.corner],
        4: [lambda: gather.forward(3)],
        5: [lambda: gather.corner(0), lambda: gather.corner(1)],
        6: [lambda: gather.corner(2)],
        7: [lambda: gather.corner(3)],
    }
    for s in range(steps):

        @pl.when(is_inner)
        def _():
            line.relay(s)
            line.relay_back(s)
            src = keep(s, line.inner_total(s))
            spread.cross_one(s, src).start()
            spread.out_any(1, s, src).start()

        @pl.when(is_end)
        def _():
            if s + 2 < steps:
                line.send_start(s + 2)
            src = keep(s, line.end_total(s))
            spread.in_zero(s, src).start()

        put_own(s).start()
        if s >= 1:
            hand_on(s - 1)
        for job in jobs.get(s, ()):
            job()
    hand_on(steps - 1)
    gather.finish()
    down_part.finish()
    for s in range(steps):
        put_own(s).wait()

        @pl.when(is_end)
        def _():
            for o in (1, 2, 3):
                spread.out_any(o, s).wait_recv()
            line.finish_end(s)
            spread.in_zero(s).wait_send()

        @pl.when(is_inner)
        def _():
            line.finish_inner(s)
            spread.cross_one(s).wait_send()
            spread.cross_zero(s).wait_send()
            for o in (1, 2, 3):
                spread.out_any(o, s).wait_send()


def middle(terms, tokens, w, down_src):
    side = lax.axis_size("tp")
    count, width = terms.shape
    own = count // lax.axis_size("fs")
    down = jax.ShapeDtypeStruct((down_src.shape[0], down_src.shape[1] * side), down_src.dtype)
    return pl.pallas_call(
        middle_kernel,
        out_shape=(
            jax.ShapeDtypeStruct(terms.shape, terms.dtype),
            jax.ShapeDtypeStruct(w.shape, w.dtype),
            down,
        ),
        in_specs=[VMEM, ANY, ANY, ANY],
        out_specs=(ANY,) * 3,
        input_output_aliases={2: 1},
        scratch_shapes=[
            pltpu.VMEM((own, width), jnp.bfloat16),
            pltpu.VMEM((own, width), jnp.bfloat16),
            pltpu.VMEM(down_src.shape, down_src.dtype),
            *line_scratch(own, width),
            pltpu.SemaphoreType.DMA((2, LineSpread.kinds, steps)),
            pltpu.SemaphoreType.DMA((2, side, PlaneGather.kinds)),
            pltpu.SemaphoreType.DMA((2, DownGather.kinds)),
            pltpu.SemaphoreType.DMA((3 + steps,)),
        ],
        compiler_params=pltpu.CompilerParams(
            has_side_effects=True, vmem_limit_bytes=48 * 1024 * 1024
        ),
        name="sum_norm_spread",
    )(terms, tokens, w, down_src)


def last_kernel(
    terms, normed, gain, result,
    own_rows, from_outer, from_inner, from_middle, to_inner, to_outer, line_sems, local,
):
    h = Here()
    own = result.shape[0]
    size = own // steps
    is_end = h.end == 0
    is_inner = h.end == 1
    line = LineSum(h, terms, from_outer, from_inner, from_middle, to_inner, to_outer, line_sems)

    @pl.when(is_end)
    def _():
        for s in range(steps):
            line.send_start(s)

    take = pltpu.make_async_copy(
        normed.at[pl.ds(pl.multiple_of(h.f * own, own), own)], own_rows, local.at[0]
    )
    take.start()
    take.wait()

    def keep(s, total):
        at = pl.ds(s * size, size)
        residual = deep_alpha * gain[...] * own_rows[at, :].astype(jnp.float32)
        result[at, :] = plain_norm(residual + half_step * total).astype(jnp.bfloat16)

    for s in range(steps):

        @pl.when(is_inner)
        def _():
            line.relay(s)
            line.relay_back(s)
            keep(s, line.inner_total(s))

        @pl.when(is_end)
        def _():
            keep(s, line.end_total(s))

    for s in range(steps):

        @pl.when(is_end)
        def _():
            line.finish_end(s)

        @pl.when(is_inner)
        def _():
            line.finish_inner(s)


def last(terms, normed, gain):
    count, width = terms.shape
    own = count // lax.axis_size("fs")
    return pl.pallas_call(
        last_kernel,
        out_shape=jax.ShapeDtypeStruct((own, width), jnp.bfloat16),
        in_specs=[VMEM, ANY, VMEM],
        out_specs=VMEM,
        scratch_shapes=[
            pltpu.VMEM((own, width), jnp.bfloat16),
            *line_scratch(own, width),
            pltpu.SemaphoreType.DMA((1,)),
        ],
        compiler_params=pltpu.CompilerParams(
            has_side_effects=True, vmem_limit_bytes=48 * 1024 * 1024
        ),
        name="sum_norm_last",
    )(terms, normed, gain)


def body(prompt, gate_first, up_first, down_first, norm_gain, gate_second, up_second, down_second):
    side, groups, planes = lax.axis_size("tp"), lax.axis_size("grp"), lax.axis_size("fs")
    fs_index = lax.axis_index("fs")
    tokens = prompt.reshape(-1, prompt.shape[-1])
    row_block, width = gate_first.shape
    gain_rows = lax.dynamic_slice_in_dim(norm_gain, fs_index * row_block, row_block, 0)[:, None]
    down_a, down_b = down_first.astype(jnp.bfloat16), down_second.astype(jnp.bfloat16)
    planar = (
        groups == 2
        and side == 2 * groups
        and planes == side
        and row_block % (4 * 64) == 0
        and width % lane == 0
        and down_first.shape[0] % 32 == 0
        and down_first.shape[1] % lane == 0
        and tokens.shape[0] % (planes * steps * 16) == 0
        and tokens.shape[1] % (2 * lane) == 0
    )
    if planar:
        src_one = jnp.stack([gate_first.astype(jnp.bfloat16), up_first.astype(jnp.bfloat16)])
        src_two = jnp.stack(
            [
                (gain_rows * gate_second).astype(jnp.bfloat16),
                (gain_rows * up_second).astype(jnp.bfloat16),
            ]
        )
        w_one, down_one, w_two = gather_weights(src_one, down_a, src_two)
        terms_one, gate_one, up_one, down_one = compute_terms(tokens, w_one, down_one)
        normed, w_two, down_two = middle(terms_one, tokens, w_two, down_b)
        terms_two, gate_two, up_two, down_two = compute_terms(normed, w_two, down_two)
        result = last(terms_two, normed, norm_gain[None, :])
    else:
        result, gate_one, up_one, down_one, gate_two, up_two, down_two = general_blocks(
            tokens,
            norm_gain,
            (gate_first.astype(jnp.bfloat16), up_first.astype(jnp.bfloat16), down_a),
            (
                (gain_rows * gate_second).astype(jnp.bfloat16),
                (gain_rows * up_second).astype(jnp.bfloat16),
                down_b,
            ),
        )
    return (
        result.reshape(1, result.shape[0], result.shape[-1]),
        gate_one,
        up_one,
        down_one,
        gate_two,
        up_two,
        down_two,
    )


def solution(mesh):
    placed = (
        P(("grp", "tp"), None, None),
        P("fs", "tp"),
        P("fs", "tp"),
        P("fs", "tp"),
        P(),
        P("fs", "tp"),
        P("fs", "tp"),
        P("fs", "tp"),
    )
    return jax.shard_map(
        body,
        mesh=mesh,
        in_specs=placed,
        out_specs=(
            P(("grp", "tp"), "fs", None),
            P("grp", "fs"),
            P("grp", "fs"),
            P("fs", "grp"),
            P("grp", "fs"),
            P("grp", "fs"),
            P("fs", "grp"),
        ),
        check_vma=False,
    )
```

profile of v0, /device:TPU:0, one launch (start us, length us, event | category | flops | bytes accessed | tf_op | source)
XLA Modules:
  0.0 449.8 jit_solution(10286074384976072319)
XLA Ops:
  0.6 0.0 copy-start.5
  0.6 0.9 dynamic_slice.3
  1.6 0.0 copy-start.4
  1.6 3.3 convert_element_type.20.down_src
  4.8 0.0 copy-done.5
  4.8 0.0 copy-start.3
  4.8 0.2 convert_element_type.23.down_src
  5.0 0.0 copy-done.4
  5.0 1.6 copy-done.3
  6.6 0.6 fusion
  7.3 0.0 copy-start.6
  7.3 0.0 copy-start.7
  7.3 1.9 pad_maximum_fusion.1.src_two
  9.2 1.0 copy-done.6
  10.1 0.9 copy-done.7
  11.0 0.3 convert_bitcast_fusion
  11.3 1.9 pad_maximum_fusion.src_one
  13.2 121.9 %gather_weights.1 = (bf16[2,2048,1408]{2,1,0:T(8,128)(2,1)}, bf16[1408,2048]{1,0:T(8,128)(2,1)}, bf16[2,2048,1408]{2,1,0:T(8,128)(2,1)}) custom-call(bf16[2,512,1408]{2,1,0:T(8,128)(2,1)} %pad_maximum_fusion.src_one, bf16[1408,512]{1,0:T(8,128)(2,1)} %convert_element_type.20.down_src, bf16[2,512,1408]{2,1,0:T(8,128)(2,1)} %pad_maximum_fusion.1.src_two), custom_call_target="tpu_custom_call" | custom-call | tf_op jit(solution)/shard_map/gather_weights/pallas_call | solution.py:345
  135.1 37.9 %compute_terms.2 = (bf16[1024,2048]{1,0:T(8,128)(2,1)}, bf16[2048,1408]{1,0:T(8,128)(2,1)}, bf16[2048,1408]{1,0:T(8,128)(2,1)}, bf16[1408,2048]{1,0:T(8,128)(2,1)}) custom-call(bf16[1024,2048]{1,0:T(8,128)(2,1)} %bitcast.13, bf16[2,2048,1408]{2,1,0:T(8,128)(2,1)} %get-tuple-element.21.w, bf16[1408,2048]{1,0:T(8,128)(2,1)} %get-tuple-element.22.down), custom_call_target="tpu_custom_call" | custom-call | flops 17716740096 | bytes 34603008 | tf_op jit(solution)/shard_map/compute_terms/pallas_call | solution.py:447
  173.0 153.4 %sum_norm_spread.1 = (bf16[1024,2048]{1,0:T(8,128)(2,1)S(1)}, bf16[2,2048,1408]{2,1,0:T(8,128)(2,1)}, bf16[1408,2048]{1,0:T(8,128)(2,1)}) custom-call(bf16[1024,2048]{1,0:T(8,128)(2,1)} %get-tuple-element.23.terms, bf16[1024,2048]{1,0:T(8,128)(2,1)} %bitcast.14, bf16[2,2048,1408]{2,1,0:T(8,128)(2,1)} %get-tuple-element.24.w_in, ...), custom_call_target="tpu_custom_call", output_to_operand_aliasing={{1}: (2, {})} | custom-call | tf_op jit(solution)/shard_map/sum_norm_spread/pallas_call | solution.py:718
  326.4 0.0 copy-start
  326.4 2.0 copy-done
  328.4 0.0 copy-start.2
  328.4 37.9 %compute_terms.3 = (bf16[1024,2048]{1,0:T(8,128)(2,1)}, bf16[2048,1408]{1,0:T(8,128)(2,1)}, bf16[2048,1408]{1,0:T(8,128)(2,1)}, bf16[1408,2048]{1,0:T(8,128)(2,1)}) custom-call(bf16[1024,2048]{1,0:T(8,128)(2,1)} %copy-done, bf16[2,2048,1408]{2,1,0:T(8,128)(2,1)} %get-tuple-element.26.w, bf16[1408,2048]{1,0:T(8,128)(2,1)} %get-tuple-element.27.down), custom_call_target="tpu_custom_call" | custom-call | flops 17716740096 | bytes 34603008 | tf_op jit(solution)/shard_map/compute_terms/pallas_call | solution.py:447
  366.3 0.0 copy-done.2
  366.3 0.0 copy-start.1
  366.3 2.2 copy-done.1
  368.5 80.3 %sum_norm_last.1 = bf16[256,2048]{1,0:T(8,128)(2,1)S(1)} custom-call(bf16[1024,2048]{1,0:T(8,128)(2,1)S(1)} %copy-done.1, bf16[1024,2048]{1,0:T(8,128)(2,1)} %copy-done, f32[1,2048]{1,0:T(1,128)S(1)} %bitcast.12), custom_call_target="tpu_custom_call" | custom-call | tf_op jit(solution)/shard_map/sum_norm_last/pallas_call | solution.py:798
  448.9 1.0 copy.18
Async XLA Ops:
  0.6 4.2 copy-start.5
  1.6 3.4 copy-start.4
  4.8 1.8 copy-start.3
  7.3 2.9 copy-start.6
  7.3 3.7 copy-start.7
  326.4 2.0 copy-start
  328.4 37.9 %copy-start.2 = (f32[2048]{0:T(1024)S(1)}, f32[2048]{0:T(1024)}, u32[]{:S(2)}) copy-start(f32[2048]{0:T(1024)} %param.12) | copy-start | bytes 24580
  366.3 2.2 copy-start.1
where the time goes:
time: 450 us
  Pallas kernels  431 us (96%)
  local copies, waits for them, and re-layouts  9.51 us (2%)
  other arithmetic  8.1 us (2%)
    pallas_call x1, Pallas kernels, middle(): pl.pallas_call(middle_kernel, out_shape=(jax.ShapeDtypeStruct(terms.shape...  153 us
    pallas_call x1, Pallas kernels, gather_weights(): pl.pallas_call(weights_kernel, out_shape=(full, down, full), in_specs=[AN...  122 us
    pallas_call x1, Pallas kernels, last(): pl.pallas_call(last_kernel, out_shape=jax.ShapeDtypeStruct((own, width),...  80.3 us
    pallas_call x2, Pallas kernels, compute_terms(): pl.pallas_call(compute_kernel, out_shape=(jax.ShapeDtypeStruct((count, do...  75.8 us

commit v1 on v0

v1 whole, which is shorter than its diff:
```python
import jax
import jax.numpy as jnp
from jax import lax
from jax.experimental import pallas as pl
from jax.experimental.pallas import tpu as pltpu
from jax.sharding import PartitionSpec as P

norm_eps = 1e-05
deep_alpha = 2.0**0.25
half_step = 0.5
lane = 128
steps = 4
MESH = pl.DeviceIdType.MESH
ANY = pl.BlockSpec(memory_space=pl.ANY)
VMEM = pl.BlockSpec(memory_space=pltpu.VMEM)


def plain_norm(values):
    row_mean = jnp.mean(values, axis=-1, keepdims=True)
    centred = values - row_mean
    variance = jnp.mean(centred * centred, axis=-1, keepdims=True)
    return centred * lax.rsqrt(variance + norm_eps)


def gated_hidden(inputs, gate_proj, up_proj):
    gate_act = jnp.dot(inputs, gate_proj, preferred_element_type=jnp.float32)
    up_act = jnp.dot(inputs, up_proj, preferred_element_type=jnp.float32)
    return (jax.nn.silu(gate_act) * up_act).astype(jnp.bfloat16)


def relay_weights(gate_proj, up_proj, down_proj):
    gate_rows, up_rows, down_mine = (
        lax.all_gather(gate_proj, "tp", axis=1, tiled=True),
        lax.all_gather(up_proj, "tp", axis=1, tiled=True),
        lax.all_gather(down_proj, "tp", axis=1, tiled=True),
    )
    gate_mine, up_mine = (
        lax.all_to_all(gate_rows, "fs", split_axis=1, concat_axis=0, tiled=True),
        lax.all_to_all(up_rows, "fs", split_axis=1, concat_axis=0, tiled=True),
    )
    return (gate_mine, up_mine, down_mine)


def general_blocks(tokens, norm_gain, first, second):
    fs_index, fs_count = lax.axis_index("fs"), lax.axis_size("fs")
    own_count = tokens.shape[0] // fs_count

    def summed(rows, projs):
        terms = jnp.dot(
            gated_hidden(rows, projs[0], projs[1]), projs[2], preferred_element_type=jnp.float32
        ).astype(jnp.bfloat16)
        parts = lax.all_to_all(
            terms.reshape(fs_count, own_count, -1), "fs", split_axis=0, concat_axis=0
        )
        return jnp.sum(parts.astype(jnp.float32), axis=0)

    own_tokens = lax.dynamic_slice_in_dim(tokens, fs_index * own_count, own_count, 0)
    first = relay_weights(*first)
    second = relay_weights(*second)
    normed_own = plain_norm(
        deep_alpha * own_tokens.astype(jnp.float32) + half_step * summed(tokens, first)
    ).astype(jnp.bfloat16)
    normed = lax.all_gather(normed_own, "fs", axis=0, tiled=True)
    ffn_two = summed(normed, second)
    residual_two = deep_alpha * norm_gain * normed_own.astype(jnp.float32)
    return (plain_norm(residual_two + half_step * ffn_two).astype(jnp.bfloat16), *first, *second)


class Here:
    def __init__(self):
        self.g, self.f, self.t = (lax.axis_index(name) for name in ("grp", "fs", "tp"))
        side = lax.axis_size("tp")
        self.side = side
        self.x, self.c = self.t // 2, self.t % 2
        self.q = self.g * 2 + self.x
        self.xt = (self.t + 2) % side
        self.ct = self.t + 1 - 2 * self.c
        self.xn = (self.g, self.f, self.xt)
        self.yn = (1 - self.g, self.f, self.t)
        self.cn = (self.g, self.f, self.ct)
        last = lax.axis_size("fs") - 1
        self.m = self.f // 2
        self.end = self.f + self.m * (last - 2 * self.f)
        self.inner = (self.g, self.f + 1 - 2 * self.m, self.t)
        self.outer = (self.g, self.f - 1 + 2 * self.m, self.t)
        self.last = last

    def owner(self, mirrored):
        return mirrored + self.m * (self.last - 2 * mirrored)

    def order(self, k):
        f = self.f
        return (f, f + 1 - 2 * (f % 2), (f + 2) % self.side, self.last - f)[k]


def remote(src, dst, send_sem, recv_sem, device):
    return pltpu.make_async_remote_copy(
        src_ref=src,
        dst_ref=dst,
        send_sem=send_sem,
        recv_sem=recv_sem,
        device_id=device,
        device_id_type=MESH,
    )


class PlaneGather:
    kinds = 7

    def __init__(self, here, w, sems, cuts, over_y):
        self.h, self.w, self.sems, self.cuts, self.over_y = here, w, sems, cuts, over_y
        self.rows = w.shape[1] // here.side
        self.quarter = self.rows // 4
        self.piece = self.quarter // cuts
        self.count = cuts * here.side
        self.started = []

    def place(self, p):
        return p // self.h.side, self.h.order(p % self.h.side)

    def region(self, which, cut, z, q):
        first = z * self.rows + q * self.quarter + cut * self.piece
        return self.w.at[which, pl.ds(first, self.piece)]

    def send(self, cut, z, kind, region, device):
        copy = remote(
            region, region, self.sems.at[0, cut, z, kind], self.sems.at[1, cut, z, kind], device
        )
        copy.start()
        self.started.append(copy)

    def arrive(self, cut, z, kind, region):
        remote(
            region, region, self.sems.at[0, cut, z, kind], self.sems.at[1, cut, z, kind], self.h.cn
        ).wait_recv()

    def own(self, p):
        h = self.h
        cut, z = self.place(p)
        region = self.region(h.c, cut, z, h.q)
        self.send(cut, z, 0, region, h.xn)
        self.send(cut, z, 1, region, h.yn)
        self.send(cut, z, 3, region, h.cn)

    def quarters(self):
        h = self.h
        return (h.g * 2 + 1 - h.x, (1 - h.g) * 2 + h.x, (1 - h.g) * 2 + 1 - h.x)

    def forward(self, p):
        h = self.h
        cut, z = self.place(p)
        from_x, from_y, unused = self.quarters()
        region = self.region(h.c, cut, z, from_x)
        self.arrive(cut, z, 0, region)
        if cut < self.over_y:
            self.send(cut, z, 2, region, h.yn)
        self.send(cut, z, 4, region, h.cn)
        region = self.region(h.c, cut, z, from_y)
        self.arrive(cut, z, 1, region)
        if cut >= self.over_y:
            self.send(cut, z, 2, region, h.xn)
        self.send(cut, z, 5, region, h.cn)

    def corner(self, p):
        h = self.h
        cut, z = self.place(p)
        region = self.region(h.c, cut, z, self.quarters()[2])
        self.arrive(cut, z, 2, region)
        self.send(cut, z, 6, region, h.cn)

    def finish(self):
        h, other = self.h, 1 - self.h.c
        from_x, from_y, across = self.quarters()
        for p in range(self.count):
            cut, z = self.place(p)
            for kind, q in ((3, h.q), (4, from_x), (5, from_y), (6, across)):
                self.arrive(cut, z, kind, self.region(other, cut, z, q))

    def drain(self):
        for copy in self.started:
            copy.wait_send()


class DownGather:
    kinds = 5

    def __init__(self, here, src, dst, sems, bounce, local):
        self.h, self.src, self.dst, self.sems = here, src, dst, sems
        self.bounce, self.local = bounce, local
        self.half = src.shape[0] // 2
        self.started = []

    def part(self, g, t):
        return self.dst.at[t, pl.ds(g * self.half, self.half)]

    def send(self, kind, src, dst, device):
        copy = remote(src, dst, self.sems.at[0, kind], self.sems.at[1, kind], device)
        copy.start()
        self.started.append(copy)

    def arrive(self, kind, region):
        remote(
            region, region, self.sems.at[0, kind], self.sems.at[1, kind], self.h.cn
        ).wait_recv()

    def begin(self):
        h = self.h
        self.take = pltpu.make_async_copy(self.src, self.bounce, self.local.at[0])
        self.take.start()
        self.send(
            0, self.src.at[pl.ds(h.g * self.half, self.half)], self.part(h.g, h.t), h.xn
        )
        self.send(2, self.src, self.dst.at[h.t], h.cn)

    def place(self):
        self.take.wait()
        self.put = pltpu.make_async_copy(
            self.bounce, self.dst.at[self.h.t], self.local.at[1]
        )
        self.put.start()

    def forward(self):
        h = self.h
        region = self.part(h.g, h.xt)
        self.arrive(0, region)
        self.send(1, region, region, h.yn)
        self.send(3, region, region, h.cn)

    def corner(self):
        h = self.h
        region = self.part(1 - h.g, h.xt)
        self.arrive(1, region)
        self.send(4, region, region, h.cn)

    def finish(self):
        h = self.h
        across = (h.ct + 2) % h.side
        self.arrive(2, self.dst.at[h.ct])
        self.arrive(3, self.part(h.g, across))
        self.arrive(4, self.part(1 - h.g, across))
        self.put.wait()

    def drain(self):
        for copy in self.started:
            copy.wait_send()


class Placement:
    def __init__(self, here, src, dst, sems, stage, stage_sems, bounce, local, cuts):
        self.h, self.src, self.dst, self.cuts = here, src, dst, cuts
        self.sems, self.stage, self.stage_sems = sems, stage, stage_sems
        self.bounce, self.local = bounce, local
        self.rows = src.shape[1]
        self.quarter = self.rows // 4
        self.piece = self.quarter // cuts

    def target_rows(self, which, cut):
        h = self.h
        first = h.f * self.rows + h.q * self.quarter + cut * self.piece
        return self.dst.at[which, pl.ds(first, self.piece)]

    def direct(self, cut, c):
        h = self.h
        first = h.q * self.quarter + cut * self.piece
        copy = remote(
            self.src.at[c, pl.ds(first, self.piece)],
            self.target_rows(c, cut),
            self.sems.at[0, cut, c],
            self.sems.at[2, cut, h.f],
            (h.g, h.t, 2 * h.x + c),
        )
        return jnp.logical_and(h.f == h.t, h.c == c), copy

    def staged(self, cut):
        h = self.h
        first = (h.g * 2 + 1 - h.x) * self.quarter + cut * self.piece
        return remote(
            self.src.at[:, pl.ds(first, self.piece)],
            self.stage.at[:, pl.ds(cut * self.piece, self.piece)],
            self.stage_sems.at[0, cut],
            self.stage_sems.at[1, cut],
            h.xn,
        )

    def passed_on(self, cut, c):
        h = self.h
        copy = remote(
            self.stage.at[c, pl.ds(cut * self.piece, self.piece)],
            self.target_rows(c, cut),
            self.sems.at[1, cut, c],
            self.sems.at[2, cut, h.f],
            (h.g, h.xt, 2 * h.x + c),
        )
        return jnp.logical_and(h.f == h.xt, h.c == c), copy

    def kept(self, cut):
        h = self.h
        return pltpu.make_async_copy(
            self.stage.at[h.c, pl.ds(cut * self.piece, self.piece)],
            self.target_rows(h.c, cut),
            self.stage_sems.at[2, cut],
        )

    def begin(self):
        for cut in range(self.cuts):
            self.staged(cut).start()
            for c in range(2):
                mine, copy = self.direct(cut, c)

                @pl.when(jnp.logical_not(mine))
                def _():
                    copy.start()

    def local_copy(self):
        h = self.h
        first = h.q * self.quarter

        @pl.when(h.f == h.t)
        def _():
            take = pltpu.make_async_copy(
                self.src.at[h.c, pl.ds(first, self.quarter)], self.bounce, self.local
            )
            take.start()
            take.wait()
            put = pltpu.make_async_copy(
                self.bounce,
                self.dst.at[h.c, pl.ds(h.f * self.rows + first, self.quarter)],
                self.local,
            )
            put.start()
            put.wait()

    def relay(self, cut):
        h = self.h
        self.staged(cut).wait_recv()
        for c in range(2):
            mine, copy = self.passed_on(cut, c)

            @pl.when(jnp.logical_not(mine))
            def _():
                copy.start()

        @pl.when(h.f == h.xt)
        def _():
            self.kept(cut).start()

    def arrived(self, p):
        h = self.h
        cut, k = p // h.side, p % h.side
        z = h.order(k)
        first = z * self.rows + h.q * self.quarter + cut * self.piece
        region = self.dst.at[h.c, pl.ds(first, self.piece)]
        copy = remote(region, region, self.sems.at[0, 0, 0], self.sems.at[2, cut, z], h.cn)
        if k == 0:

            @pl.when(jnp.logical_and(h.f != h.t, h.f != h.xt))
            def _():
                copy.wait_recv()

            @pl.when(h.f == h.xt)
            def _():
                self.kept(cut).wait()

        else:
            copy.wait_recv()

    def finish(self):
        for cut in range(self.cuts):
            self.staged(cut).wait_send()
            for mine, copy in [f(cut, c) for f in (self.direct, self.passed_on) for c in range(2)]:

                @pl.when(jnp.logical_not(mine))
                def _():
                    copy.wait_send()


first_cuts = 4
second_cuts = 2


def weights_kernel(
    src_one, down_src, src_two, w_one, down_one, w_two,
    bounce, down_bounce, stage_one, stage_two, place_sems, stage_sems,
    place_sems_two, stage_sems_two, plane_sems, down_sems, local,
):
    h = Here()
    first = Placement(
        h, src_one, w_one, place_sems, stage_one, stage_sems, bounce, local.at[2], first_cuts
    )
    second = Placement(
        h, src_two, w_two, place_sems_two, stage_two, stage_sems_two, bounce, local.at[2], 1
    )
    gather = PlaneGather(h, w_one, plane_sems, first_cuts, first_cuts // 2)
    down = DownGather(h, down_src, down_one, down_sems, down_bounce, local)
    first.begin()
    down.begin()
    first.local_copy()
    first.relay(0)
    first.relay(1)
    down.place()
    side, count = h.side, gather.count
    for p in range(count + 2 * side):
        if p < count:
            first.arrived(p)
            gather.own(p)
        if 0 < p < first_cuts - 1:
            first.relay(p + 1)
        if p == side:
            down.forward()
        if side <= p < count + side:
            gather.forward(p - side)
        if p >= 2 * side:
            gather.corner(p - 2 * side)
        if p == side + 2:
            second.begin()
        if p == 3 * side:
            down.corner()
            second.relay(0)
    second.local_copy()
    gather.finish()
    down.finish()
    for p in range(side):
        second.arrived(p)
    gather.drain()
    down.drain()
    first.finish()
    second.finish()


def gather_weights(src_one, down_src, src_two):
    side = lax.axis_size("tp")
    two, rows, width = src_one.shape
    full = jax.ShapeDtypeStruct((two, rows * side, width), src_one.dtype)
    down = jax.ShapeDtypeStruct((side, *down_src.shape), down_src.dtype)
    return pl.pallas_call(
        weights_kernel,
        out_shape=(full, down, full),
        in_specs=[ANY] * 3,
        out_specs=(ANY,) * 3,
        scratch_shapes=[
            pltpu.VMEM((rows // 4, width), src_one.dtype),
            pltpu.VMEM(down_src.shape, down_src.dtype),
            pltpu.VMEM((two, rows // 4, width), src_one.dtype),
            pltpu.VMEM((two, rows // 4, width), src_one.dtype),
            pltpu.SemaphoreType.DMA((3, first_cuts, side)),
            pltpu.SemaphoreType.DMA((3, first_cuts)),
            pltpu.SemaphoreType.DMA((3, 1, side)),
            pltpu.SemaphoreType.DMA((3, 1)),
            pltpu.SemaphoreType.DMA((2, first_cuts, side, PlaneGather.kinds)),
            pltpu.SemaphoreType.DMA((2, DownGather.kinds)),
            pltpu.SemaphoreType.DMA((3,)),
        ],
        compiler_params=pltpu.CompilerParams(has_side_effects=True),
        name="gather_weights",
    )(src_one, down_src, src_two)


def gate_part(rows, w_in, j, hidden):
    act = jnp.dot(rows, w_in[j], preferred_element_type=jnp.float32)
    gate_act, up_act = act[:, :lane], act[:, lane:]
    value = gate_act / (1.0 + jnp.exp(-gate_act)) * up_act
    hidden[:, pl.ds(pl.multiple_of(j * lane, lane), lane)] = value.astype(jnp.bfloat16)


def compute_kernel(
    tokens, w, down, terms, gate_out, up_out, down_out,
    rows_in, w_in, down_in, hidden, terms_in, sems,
):
    groups = w.shape[2] // lane
    wide = 4 * lane
    spans = down_out.shape[1] // wide
    parts, unused, cols = down.shape

    def w_load(which, j):
        return pltpu.make_async_copy(
            w.at[which, :, pl.ds(pl.multiple_of(j * lane, lane), lane)],
            w_in.at[j, :, pl.ds(which * lane, lane)],
            sems.at[which, j],
        )

    def w_store(which, j):
        return pltpu.make_async_copy(
            w_in.at[j, :, pl.ds(which * lane, lane)],
            (gate_out, up_out)[which].at[:, pl.ds(pl.multiple_of(j * lane, lane), lane)],
            sems.at[2 + which, j],
        )

    take_rows = pltpu.make_async_copy(tokens, rows_in, sems.at[4, 0])
    take_down = [
        pltpu.make_async_copy(
            down.at[i], down_in.at[:, pl.ds(i * cols, cols)], sems.at[4, 3 + i]
        )
        for i in range(parts)
    ]
    give_down = pltpu.make_async_copy(down_in, down_out, sems.at[4, 1])
    take_rows.start()

    @pl.loop(0, groups)
    def _(j):
        w_load(0, j).start()
        w_load(1, j).start()

    for copy in take_down:
        copy.start()
    take_rows.wait()

    @pl.loop(0, groups)
    def _(j):
        w_load(0, j).wait()
        w_load(1, j).wait()
        w_store(0, j).start()
        w_store(1, j).start()

        gate_part(rows_in[...], w_in, j, hidden)

    for copy in take_down:
        copy.wait()
    give_down.start()

    @pl.loop(0, spans)
    def _(n):
        cols = pl.ds(pl.multiple_of(n * wide, wide), wide)

        terms_in[:, cols] = jnp.dot(
            hidden[...], down_in[:, cols], preferred_element_type=jnp.float32
        ).astype(jnp.bfloat16)

    give_terms = pltpu.make_async_copy(terms_in, terms, sems.at[4, 2])
    give_terms.start()

    @pl.loop(0, groups)
    def _(j):
        w_store(0, j).wait()
        w_store(1, j).wait()

    give_down.wait()
    give_terms.wait()


def compute_terms(tokens, w, down):
    two, depth, width = w.shape
    count = tokens.shape[0]
    groups = width // lane
    parts, down_rows, cols = down.shape
    down_shape = (down_rows, parts * cols)
    proj = jax.ShapeDtypeStruct((depth, width), w.dtype)
    flops = 2 * count * depth * width * 3
    return pl.pallas_call(
        compute_kernel,
        out_shape=(
            jax.ShapeDtypeStruct((count, parts * cols), jnp.bfloat16),
            proj,
            proj,
            jax.ShapeDtypeStruct(down_shape, down.dtype),
        ),
        in_specs=[ANY] * 3,
        out_specs=(ANY,) * 4,
        scratch_shapes=[
            pltpu.VMEM(tokens.shape, tokens.dtype),
            pltpu.VMEM((groups, depth, 2 * lane), w.dtype),
            pltpu.VMEM(down_shape, down.dtype),
            pltpu.VMEM((count, width), jnp.bfloat16),
            pltpu.VMEM((count, parts * cols), jnp.bfloat16),
            pltpu.SemaphoreType.DMA((5, max(groups, 3 + parts))),
        ],
        compiler_params=pltpu.CompilerParams(vmem_limit_bytes=56 * 1024 * 1024),
        cost_estimate=pl.CostEstimate(flops=flops, bytes_accessed=6 * w.size, transcendentals=0),
        name="compute_terms",
    )(tokens, w, down)


class LineSum:
    kinds = 6

    def __init__(self, here, terms, place, from_outer, from_inner, from_middle, to_inner, to_outer, sems):
        self.h, self.terms, self.place = here, terms, place
        self.from_outer, self.from_inner, self.from_middle = from_outer, from_inner, from_middle
        self.to_inner, self.to_outer, self.sems = to_inner, to_outer, sems
        self.own = terms.shape[0] // (here.last + 1)
        self.size = self.own // steps

    def term(self, mirrored, s):
        return self.place(self.h.owner(mirrored), s)

    def at(self, s):
        return pl.ds(pl.multiple_of(s * self.size, self.size), self.size)

    def copy(self, src, dst, kind, s, device):
        return remote(src, dst, self.sems.at[0, kind, s], self.sems.at[1, kind, s], device)

    def start_copy(self, o, s):
        slot = 3 - o
        return self.copy(
            self.terms.at[self.term(o, s)], self.from_outer.at[slot, self.at(s)], slot, s,
            self.h.inner,
        )

    def middle_copy(self, o, s):
        slot = 3 - o
        return self.copy(
            self.to_inner.at[slot, self.at(s)], self.from_middle.at[slot, self.at(s)], 3 + slot,
            s, self.h.inner,
        )

    def back_copy(self, s):
        return self.copy(
            self.to_outer.at[self.at(s)], self.from_inner.at[self.at(s)], 5, s, self.h.outer
        )

    def send_start(self, s):
        for o in (3, 2, 1):
            self.start_copy(o, s).start()

    def relay(self, s):
        at = self.at(s)
        for o in (3, 2):
            slot = 3 - o
            self.start_copy(o, s).wait_recv()
            self.to_inner[slot, at, :] = (
                self.from_outer[slot, at, :].astype(jnp.float32)
                + self.terms[self.term(o, s), :].astype(jnp.float32)
            ).astype(jnp.bfloat16)
            self.middle_copy(o, s).start()

    def relay_back(self, s):
        at = self.at(s)
        self.middle_copy(3, s).wait_recv()
        self.to_outer[at, :] = (
            self.from_middle[0, at, :].astype(jnp.float32)
            + self.terms[self.term(0, s), :].astype(jnp.float32)
        ).astype(jnp.bfloat16)
        self.back_copy(s).start()

    def inner_total(self, s):
        at = self.at(s)
        self.start_copy(1, s).wait_recv()
        self.middle_copy(2, s).wait_recv()
        return (
            self.from_outer[2, at, :].astype(jnp.float32)
            + self.terms[self.term(1, s), :].astype(jnp.float32)
        ) + self.from_middle[1, at, :].astype(jnp.float32)

    def end_total(self, s):
        at = self.at(s)
        self.back_copy(s).wait_recv()
        return self.terms[self.term(0, s), :].astype(jnp.float32) + self.from_inner[
            at, :
        ].astype(jnp.float32)

    def finish_end(self, s):
        for o in (3, 2, 1):
            self.start_copy(o, s).wait_send()

    def finish_inner(self, s):
        self.middle_copy(3, s).wait_send()
        self.middle_copy(2, s).wait_send()
        self.back_copy(s).wait_send()


def line_scratch(own, width):
    def rows(*lead):
        return pltpu.VMEM((*lead, own, width), jnp.bfloat16)

    return [
        rows(3), rows(), rows(2), rows(2), rows(),
        pltpu.SemaphoreType.DMA((2, LineSum.kinds, steps)),
    ]


class LineSpread:
    kinds = 6

    def __init__(self, here, out, place, sems):
        self.h, self.out, self.place, self.sems = here, out, place, sems

    def copy(self, mirrored, kind, s, device):
        rows = self.out.at[self.place(self.h.owner(mirrored), s)]
        return remote(
            rows, rows, self.sems.at[0, kind, s], self.sems.at[1, kind, s], device
        )

    def in_zero(self, s):
        return self.copy(0, 0, s, self.h.inner)

    def cross_one(self, s):
        return self.copy(1, 1, s, self.h.inner)

    def cross_zero(self, s):
        return self.copy(0, 2, s, self.h.inner)

    def out_any(self, o, s):
        return self.copy(o, 2 + o, s, self.h.outer)

    def hand_on(self, s):
        self.in_zero(s).wait_recv()
        self.cross_zero(s).start()
        self.copy(2, 1, s, self.h.inner).wait_recv()
        self.out_any(2, s).start()
        self.copy(3, 2, s, self.h.inner).wait_recv()
        self.out_any(3, s).start()

    def finish_inner(self, s):
        self.cross_one(s).wait_send()
        self.cross_zero(s).wait_send()
        for o in (1, 2, 3):
            self.out_any(o, s).wait_send()


halves = 2


def blocks_kernel(
    terms_one, tokens, gain, w_in, down_src, result, w, down,
    own_rows, normed, terms_two, hidden, w_held, down_held, down_bounce,
    outer_one, inner_one, middle_one, to_inner_one, to_outer_one, line_one,
    outer_two, inner_two, middle_two, to_inner_two, to_outer_two, line_two,
    spread_sems, plane_sems, down_sems, local, load_sems,
):
    h = Here()
    own, size = result.shape[0], result.shape[0] // steps
    count = normed.shape[0]
    half, per = count // halves, steps // halves
    is_end, is_inner = h.end == 0, h.end == 1

    def span(first, length):
        return pl.ds(pl.multiple_of(first, size), length)

    def plain_place(owner, s):
        return span(owner * own + s * size, size)

    def half_place(owner, s):
        return span((s // per) * half + owner * (own // halves) + (s % per) * size, size)

    one = LineSum(
        h, terms_one, plain_place, outer_one, inner_one, middle_one, to_inner_one, to_outer_one,
        line_one,
    )
    two = LineSum(
        h, terms_two, half_place, outer_two, inner_two, middle_two, to_inner_two, to_outer_two,
        line_two,
    )
    spread = LineSpread(h, normed, half_place, spread_sems)
    gather = PlaneGather(h, w, plane_sems, second_cuts, 1)
    down_part = DownGather(h, down_src, down, down_sems, down_bounce, local)
    take = pltpu.make_async_copy(tokens.at[span(h.f * own, own)], own_rows, local.at[2])
    take.start()

    @pl.when(is_end)
    def _():
        one.send_start(0)

    for p in range(gather.count):
        gather.own(p)
    down_part.begin()
    down_part.place()
    take.wait()

    def keep_one(s, total):
        at = pl.ds(s * size, size)
        normed[half_place(h.f, s), :] = plain_norm(
            deep_alpha * own_rows[at, :].astype(jnp.float32) + half_step * total
        ).astype(jnp.bfloat16)

    def keep_two(s, total):
        residual = deep_alpha * gain[...] * normed[half_place(h.f, s), :].astype(jnp.float32)
        result[pl.ds(s * size, size), :] = plain_norm(residual + half_step * total).astype(
            jnp.bfloat16
        )

    groups = w.shape[2] // lane
    wide = 4 * lane

    def w_load(which, j):
        return pltpu.make_async_copy(
            w.at[which, :, pl.ds(pl.multiple_of(j * lane, lane), lane)],
            w_held.at[j, :, pl.ds(which * lane, lane)],
            load_sems.at[which, j],
        )

    cols = down.shape[2]
    down_load = [
        pltpu.make_async_copy(
            down.at[i], down_held.at[:, pl.ds(i * cols, cols)], local.at[3 + i]
        )
        for i in range(h.side)
    ]

    def load():
        gather.finish()
        down_part.finish()

        @pl.loop(0, groups)
        def _(j):
            w_load(0, j).start()
            w_load(1, j).start()

        for copy in down_load:
            copy.start()

    def hide(part, first, last, wait=False):
        rows = normed.at[pl.ds(part * half, half)]

        @pl.loop(first, last)
        def _(j):
            if wait:
                w_load(0, j).wait()
                w_load(1, j).wait()
            gate_part(rows[...], w_held, j, hidden)

    def sink(part):
        @pl.loop(0, down_held.shape[1] // wide)
        def _(n):
            cols = pl.ds(pl.multiple_of(n * wide, wide), wide)
            terms_two[pl.ds(part * half, half), cols] = jnp.dot(
                hidden[...], down_held[:, cols], preferred_element_type=jnp.float32
            ).astype(jnp.bfloat16)

    def spread_end(first, last):
        @pl.when(is_end)
        def _():
            for s in range(first, last):
                for o in (1, 2, 3):
                    spread.out_any(o, s).wait_recv()

    def send_two(first, last):
        @pl.when(is_end)
        def _():
            for s in range(first, last):
                two.send_start(s)

    def relay_two(s):
        @pl.when(is_inner)
        def _():
            two.relay(s)
            two.relay_back(s)
            keep_two(s, two.inner_total(s))

    def forward(first, last):
        return [lambda p=p: gather.forward(p) for p in range(first, last)]

    def corner(first, last):
        return [lambda p=p: gather.corner(p) for p in range(first, last)]

    cut = (groups + 1) // 2
    jobs = {
        1: forward(0, 6),
        2: [*forward(6, 8), *corner(0, 4), down_part.forward],
        3: [
            *corner(4, 8),
            down_part.corner,
            load,
            lambda: spread_end(0, per),
            lambda: hide(0, 0, cut, True),
        ],
    }
    for s in range(steps):

        @pl.when(is_inner)
        def _():
            one.relay(s)
            one.relay_back(s)
            keep_one(s, one.inner_total(s))
            spread.cross_one(s).start()
            spread.out_any(1, s).start()
            if s >= 1:
                spread.hand_on(s - 1)

        @pl.when(is_end)
        def _():
            if s + 1 < steps:
                one.send_start(s + 1)
            keep_one(s, one.end_total(s))
            spread.in_zero(s).start()

        for job in jobs.get(s, ()):
            job()

    @pl.when(is_inner)
    def _():
        spread.hand_on(steps - 1)

    hide(0, cut, groups, True)
    for copy in down_load:
        copy.wait()
    sink(0)
    send_two(0, per)
    spread_end(per, steps)
    hide(1, 0, cut)
    relay_two(0)
    hide(1, cut, groups)
    relay_two(1)
    sink(1)
    send_two(per, steps)
    for s in range(2, steps):
        relay_two(s)

    @pl.when(is_end)
    def _():
        for s in range(steps):
            keep_two(s, two.end_total(s))

    gather.drain()
    down_part.drain()
    for s in range(steps):

        @pl.when(is_end)
        def _():
            one.finish_end(s)
            two.finish_end(s)
            spread.in_zero(s).wait_send()

        @pl.when(is_inner)
        def _():
            one.finish_inner(s)
            two.finish_inner(s)
            spread.finish_inner(s)


def blocks(terms, tokens, gain, w, down_src):
    side = lax.axis_size("tp")
    count, width = terms.shape
    own = count // lax.axis_size("fs")
    two, depth, hidden = w.shape
    groups = hidden // lane
    down_rows, cols = down_src.shape
    return pl.pallas_call(
        blocks_kernel,
        out_shape=(
            jax.ShapeDtypeStruct((own, width), jnp.bfloat16),
            jax.ShapeDtypeStruct(w.shape, w.dtype),
            jax.ShapeDtypeStruct((side, down_rows, cols), down_src.dtype),
        ),
        in_specs=[VMEM, ANY, VMEM, ANY, ANY],
        out_specs=(VMEM, ANY, ANY),
        input_output_aliases={3: 1},
        scratch_shapes=[
            pltpu.VMEM((own, width), jnp.bfloat16),
            pltpu.VMEM((count, width), jnp.bfloat16),
            pltpu.VMEM((count, width), jnp.bfloat16),
            pltpu.VMEM((count // halves, hidden), jnp.bfloat16),
            pltpu.VMEM((groups, depth, two * lane), w.dtype),
            pltpu.VMEM((down_rows, side * cols), down_src.dtype),
            pltpu.VMEM(down_src.shape, down_src.dtype),
            *line_scratch(own, width),
            *line_scratch(own, width),
            pltpu.SemaphoreType.DMA((2, LineSpread.kinds, steps)),
            pltpu.SemaphoreType.DMA((2, second_cuts, side, PlaneGather.kinds)),
            pltpu.SemaphoreType.DMA((2, DownGather.kinds)),
            pltpu.SemaphoreType.DMA((3 + side,)),
            pltpu.SemaphoreType.DMA((2, groups)),
        ],
        compiler_params=pltpu.CompilerParams(
            has_side_effects=True, vmem_limit_bytes=63 * 1024 * 1024
        ),
        name="sum_norm_blocks",
    )(terms, tokens, gain, w, down_src)


emit_cuts = 8


def emit_kernel(w, down, gate_out, up_out, down_out, w_held, down_held, sems):
    rows = w.shape[1] // emit_cuts
    parts, unused, cols = down.shape
    moves = []
    for i in range(parts):
        at = pl.ds(i * cols, cols)
        moves.append((down.at[i], down_held.at[:, at], down_out.at[:, at]))
    for i in range(emit_cuts):
        at = pl.ds(i * rows, rows)
        for which, out in enumerate((gate_out, up_out)):
            moves.append((w.at[which, at], w_held.at[which, at], out.at[at]))
    takes = [pltpu.make_async_copy(m[0], m[1], sems.at[0, i]) for i, m in enumerate(moves)]
    gives = [pltpu.make_async_copy(m[1], m[2], sems.at[1, i]) for i, m in enumerate(moves)]
    for take in takes:
        take.start()
    for take, give in zip(takes, gives):
        take.wait()
        give.start()
    for give in gives:
        give.wait()


def emit(w, down):
    two, depth, width = w.shape
    parts, down_rows, cols = down.shape
    proj = jax.ShapeDtypeStruct((depth, width), w.dtype)
    down_shape = (down_rows, parts * cols)
    return pl.pallas_call(
        emit_kernel,
        out_shape=(proj, proj, jax.ShapeDtypeStruct(down_shape, down.dtype)),
        in_specs=[ANY] * 2,
        out_specs=(ANY,) * 3,
        scratch_shapes=[
            pltpu.VMEM(w.shape, w.dtype),
            pltpu.VMEM(down_shape, down.dtype),
            pltpu.SemaphoreType.DMA((2, two * emit_cuts + parts)),
        ],
        compiler_params=pltpu.CompilerParams(vmem_limit_bytes=56 * 1024 * 1024),
        name="emit_projections",
    )(w, down)


def body(prompt, gate_first, up_first, down_first, norm_gain, gate_second, up_second, down_second):
    side, groups, planes = lax.axis_size("tp"), lax.axis_size("grp"), lax.axis_size("fs")
    fs_index = lax.axis_index("fs")
    tokens = prompt.reshape(-1, prompt.shape[-1])
    row_block, width = gate_first.shape
    gain_rows = lax.dynamic_slice_in_dim(norm_gain, fs_index * row_block, row_block, 0)[:, None]
    down_a, down_b = down_first.astype(jnp.bfloat16), down_second.astype(jnp.bfloat16)
    planar = (
        groups == 2
        and side == 2 * groups
        and planes == side
        and row_block % (4 * 64) == 0
        and width % lane == 0
        and down_first.shape[0] % 32 == 0
        and down_first.shape[1] % lane == 0
        and tokens.shape[0] % (planes * steps * 16) == 0
        and tokens.shape[0] % (halves * planes * 16) == 0
        and tokens.shape[1] % (4 * lane) == 0
    )
    if planar:
        src_one = jnp.stack([gate_first.astype(jnp.bfloat16), up_first.astype(jnp.bfloat16)])
        src_two = jnp.stack(
            [
                (gain_rows * gate_second).astype(jnp.bfloat16),
                (gain_rows * up_second).astype(jnp.bfloat16),
            ]
        )
        w_one, down_one, w_two = gather_weights(src_one, down_a, src_two)
        terms_one, gate_one, up_one, down_one = compute_terms(tokens, w_one, down_one)
        result, w_two, down_two = blocks(terms_one, tokens, norm_gain[None, :], w_two, down_b)
        gate_two, up_two, down_two = emit(w_two, down_two)
    else:
        result, gate_one, up_one, down_one, gate_two, up_two, down_two = general_blocks(
            tokens,
            norm_gain,
            (gate_first.astype(jnp.bfloat16), up_first.astype(jnp.bfloat16), down_a),
            (
                (gain_rows * gate_second).astype(jnp.bfloat16),
                (gain_rows * up_second).astype(jnp.bfloat16),
                down_b,
            ),
        )
    return (
        result.reshape(1, result.shape[0], result.shape[-1]),
        gate_one,
        up_one,
        down_one,
        gate_two,
        up_two,
        down_two,
    )


def solution(mesh):
    placed = (
        P(("grp", "tp"), None, None),
        P("fs", "tp"),
        P("fs", "tp"),
        P("fs", "tp"),
        P(),
        P("fs", "tp"),
        P("fs", "tp"),
        P("fs", "tp"),
    )
    return jax.shard_map(
        body,
        mesh=mesh,
        in_specs=placed,
        out_specs=(
            P(("grp", "tp"), "fs", None),
            P("grp", "fs"),
            P("grp", "fs"),
            P("fs", "grp"),
            P("grp", "fs"),
            P("grp", "fs"),
            P("fs", "grp"),
        ),
        check_vma=False,
    )
```

time: 450 us -> 354 us (0.79)
  Pallas kernels: 431 us -> 339 us
  local copies, waits for them, and re-layouts: 9.51 us -> 4.72 us
    pallas_call x4 -> x3, Pallas kernels: 310 us -> 232 us  [the longest x1 193 us: blocks(): pl.pallas_call(blocks_kernel, out_shape=(jax.ShapeDtypeStruct((own, width...]
    pallas_call x1, Pallas kernels: 122 us -> 108 us  [gather_weights(): pl.pallas_call(weights_kernel, out_shape=(full, down, full), in_specs=[AN...]
    unnamed x17 -> x13, local copies, waits for them, and re-layouts: 8.59 us -> 3.81 us
where the time goes in v1:
time: 354 us
  Pallas kernels  339 us (96%)
  other arithmetic  9.28 us (3%)
  local copies, waits for them, and re-layouts  4.72 us (1%)
    pallas_call x1, Pallas kernels, blocks(): pl.pallas_call(blocks_kernel, out_shape=(jax.ShapeDtypeStruct((own, width...  193 us
    pallas_call x1, Pallas kernels, gather_weights(): pl.pallas_call(weights_kernel, out_shape=(full, down, full), in_specs=[AN...  108 us
    pallas_call x1, Pallas kernels, compute_terms(): pl.pallas_call(compute_kernel, out_shape=(jax.ShapeDtypeStruct((count, pa...  26.1 us
    pallas_call x1, Pallas kernels, emit(): pl.pallas_call(emit_kernel, out_shape=(proj, proj, jax.ShapeDtypeStruct(d...  12.4 us

profile of v1, /device:TPU:0, one launch (start us, length us, event | category | flops | bytes accessed | tf_op | source)
XLA Modules:
  0.0 354.2 jit_solution(17551315684032293265)
XLA Ops:
  0.6 0.0 copy-start.2
  0.6 0.9 dynamic_slice.3
  1.6 0.0 copy-start.1
  1.6 3.3 convert_element_type.20.down_src
  4.8 0.0 copy-done.2
  4.8 0.0 copy-start
  4.8 1.4 convert_element_type.23.down_src
  6.2 0.0 copy-done.1
  6.2 1.0 copy-done
  7.2 0.6 fusion
  7.8 0.0 copy-start.3
  7.8 0.0 copy-start.4
  7.8 1.9 pad_maximum_fusion.1.src_two
  9.7 1.0 copy-done.3
  10.7 0.9 copy-done.4
  11.5 0.3 convert_bitcast_fusion
  11.8 1.9 pad_maximum_fusion.src_one
  13.7 107.8 %gather_weights.1 = (bf16[2,2048,1408]{2,1,0:T(8,128)(2,1)}, bf16[4,1408,512]{2,1,0:T(8,128)(2,1)}, bf16[2,2048,1408]{2,1,0:T(8,128)(2,1)}) custom-call(bf16[2,512,1408]{2,1,0:T(8,128)(2,1)} %pad_maximum_fusion.src_one, bf16[1408,512]{1,0:T(8,128)(2,1)} %convert_element_type.20.down_src, bf16[2,512,1408]{2,1,0:T(8,128)(2,1)} %pad_maximum_fusion.1.src_two), custom_call_target="tpu_custom_call" | custom-call | tf_op jit(solution)/shard_map/gather_weights/pallas_call | solution.py:435
  121.5 26.1 %compute_terms.1 = (bf16[1024,2048]{1,0:T(8,128)(2,1)}, bf16[2048,1408]{1,0:T(8,128)(2,1)}, bf16[2048,1408]{1,0:T(8,128)(2,1)}, bf16[1408,2048]{1,0:T(8,128)(2,1)}) custom-call(bf16[1024,2048]{1,0:T(8,128)(2,1)} %bitcast.11, bf16[2,2048,1408]{2,1,0:T(8,128)(2,1)} %get-tuple-element.20.w, bf16[4,1408,512]{2,1,0:T(8,128)(2,1)} %get-tuple-element.21.down), custom_call_target="tpu_custom_call" | custom-call | flops 17716740096 | bytes 34603008 | tf_op jit(solution)/shard_map/compute_terms/pallas_call | solution.py:548
  147.6 193.2 %sum_norm_blocks.1 = (bf16[256,2048]{1,0:T(8,128)(2,1)}, bf16[2,2048,1408]{2,1,0:T(8,128)(2,1)}, bf16[4,1408,512]{2,1,0:T(8,128)(2,1)}) custom-call(bf16[1024,2048]{1,0:T(8,128)(2,1)} %get-tuple-element.22.terms_one, bf16[1024,2048]{1,0:T(8,128)(2,1)} %bitcast.12, f32[1,2048]{1,0:T(1,128)} %bitcast.14, ...), custom_call_target="tpu_custom_call", output_to_operand_aliasing={{1}: (3, {})} | custom-call | tf_op jit(solution)/shard_map/sum_norm_blocks/pallas_call | solution.py:926
  340.8 0.0 copy-start.5
  340.8 12.4 %emit_projections.1 = (bf16[2048,1408]{1,0:T(8,128)(2,1)}, bf16[2048,1408]{1,0:T(8,128)(2,1)}, bf16[1408,2048]{1,0:T(8,128)(2,1)}) custom-call(bf16[2,2048,1408]{2,1,0:T(8,128)(2,1)} %get-tuple-element.28.w, bf16[4,1408,512]{2,1,0:T(8,128)(2,1)} %get-tuple-element.29.down), custom_call_target="tpu_custom_call" | custom-call | tf_op jit(solution)/shard_map/emit_projections/pallas_call | solution.py:989
  353.2 0.0 copy-done.5
  353.2 1.0 copy.18
Async XLA Ops:
  0.6 4.2 %copy-start.2 = (f32[1408,512]{1,0:T(8,128)S(1)}, f32[1408,512]{1,0:T(8,128)}, u32[]{:S(2)}) copy-start(f32[1408,512]{1,0:T(8,128)} %param.15) | copy-start | bytes 8650756
  1.6 4.6 %copy-start.1 = (f32[512,1408]{1,0:T(8,128)S(1)}, f32[512,1408]{1,0:T(8,128)}, u32[]{:S(2)}) copy-start(f32[512,1408]{1,0:T(8,128)} %param.14) | copy-start | bytes 8650756
  4.8 2.3 copy-start
  7.8 2.9 copy-start.3
  7.8 3.7 %copy-start.4 = (f32[512,1408]{1,0:T(8,128)S(1)}, f32[512,1408]{1,0:T(8,128)}, u32[]{:S(2)}) copy-start(f32[512,1408]{1,0:T(8,128)} %param.9) | copy-start | bytes 8650756
  340.8 12.4 %copy-start.5 = (bf16[256,2048]{1,0:T(8,128)(2,1)S(1)}, bf16[256,2048]{1,0:T(8,128)(2,1)}, u32[]{:S(2)}) copy-start(bf16[256,2048]{1,0:T(8,128)(2,1)} %get-tuple-element.24) | copy-start | bytes 3145732

commit v2 on v1

--- a/solution.py
+++ b/solution.py
@@ -317,13 +317,14 @@
 
         @pl.when(h.f == h.t)
         def _():
-            take = pltpu.make_async_copy(
-                self.src.at[h.c, pl.ds(first, self.quarter)], self.bounce, self.local
-            )
-            take.start()
-            take.wait()
+            held = self.src.at[h.c, pl.ds(first, self.quarter)]
+            if self.bounce is not None:
+                take = pltpu.make_async_copy(held, self.bounce, self.local)
+                take.start()
+                take.wait()
+                held = self.bounce
             put = pltpu.make_async_copy(
-                self.bounce,
+                held,
                 self.dst.at[h.c, pl.ds(h.f * self.rows + first, self.quarter)],
                 self.local,
             )
@@ -379,8 +380,8 @@
 
 
 def weights_kernel(
-    src_one, down_src, src_two, w_one, down_one, w_two,
-    bounce, down_bounce, stage_one, stage_two, place_sems, stage_sems,
+    src_one, down_src, gate_two, up_two, gain, w_one, down_one, w_two,
+    raw_two, src_two, bounce, down_bounce, stage_one, stage_two, place_sems, stage_sems,
     place_sems_two, stage_sems_two, plane_sems, down_sems, local,
 ):
     h = Here()
@@ -388,16 +389,32 @@
         h, src_one, w_one, place_sems, stage_one, stage_sems, bounce, local.at[2], first_cuts
     )
     second = Placement(
-        h, src_two, w_two, place_sems_two, stage_two, stage_sems_two, bounce, local.at[2], 1
+        h, src_two, w_two, place_sems_two, stage_two, stage_sems_two, None, local.at[2], 1
     )
     gather = PlaneGather(h, w_one, plane_sems, first_cuts, first_cuts // 2)
     down = DownGather(h, down_src, down_one, down_sems, down_bounce, local)
+    takes = [
+        pltpu.make_async_copy(proj, raw_two.at[i], local.at[3 + i])
+        for i, proj in enumerate((gate_two, up_two))
+    ]
     first.begin()
     down.begin()
+    for copy in takes:
+        copy.start()
     first.local_copy()
     first.relay(0)
     first.relay(1)
     down.place()
+    for copy in takes:
+        copy.wait()
+    block = lane // 2
+
+    @pl.loop(0, src_two.shape[1] // block)
+    def _(i):
+        at = pl.ds(pl.multiple_of(i * block, block), block)
+        for which in range(2):
+            src_two[which, at, :] = (gain[at, :] * raw_two[which, at, :]).astype(jnp.bfloat16)
+
     side, count = h.side, gather.count
     for p in range(count + 2 * side):
         if p < count:
@@ -427,7 +444,7 @@
     second.finish()
 
 
-def gather_weights(src_one, down_src, src_two):
+def gather_weights(src_one, down_src, gate_two, up_two, gain):
     side = lax.axis_size("tp")
     two, rows, width = src_one.shape
     full = jax.ShapeDtypeStruct((two, rows * side, width), src_one.dtype)
@@ -435,9 +452,11 @@
     return pl.pallas_call(
         weights_kernel,
         out_shape=(full, down, full),
-        in_specs=[ANY] * 3,
+        in_specs=[ANY, ANY, ANY, ANY, VMEM],
         out_specs=(ANY,) * 3,
         scratch_shapes=[
+            pltpu.VMEM((two, rows, width), gate_two.dtype),
+            pltpu.VMEM((two, rows, width), src_one.dtype),
             pltpu.VMEM((rows // 4, width), src_one.dtype),
             pltpu.VMEM(down_src.shape, down_src.dtype),
             pltpu.VMEM((two, rows // 4, width), src_one.dtype),
@@ -448,11 +467,13 @@
             pltpu.SemaphoreType.DMA((3, 1)),
             pltpu.SemaphoreType.DMA((2, first_cuts, side, PlaneGather.kinds)),
             pltpu.SemaphoreType.DMA((2, DownGather.kinds)),
-            pltpu.SemaphoreType.DMA((3,)),
+            pltpu.SemaphoreType.DMA((5,)),
         ],
-        compiler_params=pltpu.CompilerParams(has_side_effects=True),
+        compiler_params=pltpu.CompilerParams(
+            has_side_effects=True, vmem_limit_bytes=48 * 1024 * 1024
+        ),
         name="gather_weights",
-    )(src_one, down_src, src_two)
+    )(src_one, down_src, gate_two, up_two, gain)
 
 
 def gate_part(rows, w_in, j, hidden):
@@ -842,44 +863,71 @@
         return [lambda p=p: gather.corner(p) for p in range(first, last)]
 
     cut = (groups + 1) // 2
+    third = (groups + 3) // 4
     jobs = {
-        1: forward(0, 6),
-        2: [*forward(6, 8), *corner(0, 4), down_part.forward],
-        3: [
-            *corner(4, 8),
-            down_part.corner,
-            load,
-            lambda: spread_end(0, per),
-            lambda: hide(0, 0, cut, True),
-        ],
+        1: forward(0, 1),
+        2: forward(1, 2),
+        3: forward(2, 4),
+        4: forward(4, 5),
+        5: forward(5, 6),
+        6: forward(6, 8),
+        7: [down_part.forward, *corner(0, 2)],
+        8: corner(2, 4),
+        9: corner(4, 6),
+        10: corner(6, 8),
+        12: [down_part.corner, load],
+        13: [lambda: spread_end(0, per), lambda: hide(0, 0, third, True)],
+        14: [lambda: hide(0, third, 2 * third, True)],
+        15: [lambda: hide(0, 2 * third, groups, True)],
     }
+
+    def other(slot):
+        for job in jobs.get(slot, ()):
+            job()
+
     for s in range(steps):
 
         @pl.when(is_inner)
         def _():
             one.relay(s)
-            one.relay_back(s)
-            keep_one(s, one.inner_total(s))
-            spread.cross_one(s).start()
-            spread.out_any(1, s).start()
-            if s >= 1:
-                spread.hand_on(s - 1)
 
         @pl.when(is_end)
         def _():
             if s + 1 < steps:
                 one.send_start(s + 1)
+
+        other(4 * s)
+
+        @pl.when(is_inner)
+        def _():
+            one.relay_back(s)
+
+        other(4 * s + 1)
+
+        @pl.when(is_inner)
+        def _():
+            keep_one(s, one.inner_total(s))
+            spread.cross_one(s).start()
+            spread.out_any(1, s).start()
+
+        @pl.when(is_end)
+        def _():
             keep_one(s, one.end_total(s))
             spread.in_zero(s).start()
 
-        for job in jobs.get(s, ()):
-            job()
+        other(4 * s + 2)
+        if s >= 1:
+
+            @pl.when(is_inner)
+            def _():
+                spread.hand_on(s - 1)
+
+        other(4 * s + 3)
 
     @pl.when(is_inner)
     def _():
         spread.hand_on(steps - 1)
 
-    hide(0, cut, groups, True)
     for copy in down_load:
         copy.wait()
     sink(0)
@@ -1022,13 +1070,9 @@
     )
     if planar:
         src_one = jnp.stack([gate_first.astype(jnp.bfloat16), up_first.astype(jnp.bfloat16)])
-        src_two = jnp.stack(
-            [
-                (gain_rows * gate_second).astype(jnp.bfloat16),
-                (gain_rows * up_second).astype(jnp.bfloat16),
-            ]
-        )
-        w_one, down_one, w_two = gather_weights(src_one, down_a, src_two)
+        w_one, down_one, w_two = gather_weights(
+            src_one, down_a, gate_second, up_second, gain_rows
+        )
         terms_one, gate_one, up_one, down_one = compute_terms(tokens, w_one, down_one)
         result, w_two, down_two = blocks(terms_one, tokens, norm_gain[None, :], w_two, down_b)
         gate_two, up_two, down_two = emit(w_two, down_two)

time: 354 us -> 335 us (0.946)
  Pallas kernels: 339 us -> 327 us
  other arithmetic: 9.28 us -> 4.02 us
    pallas_call x1, Pallas kernels: 193 us -> 181 us  [blocks(): pl.pallas_call(blocks_kernel, out_shape=(jax.ShapeDtypeStruct((own, width...]
where the time goes in v2:
time: 335 us
  Pallas kernels  327 us (98%)
  other arithmetic  4.02 us (1%)
    pallas_call x1, Pallas kernels, blocks(): pl.pallas_call(blocks_kernel, out_shape=(jax.ShapeDtypeStruct((own, width...  181 us
    pallas_call x1, Pallas kernels, gather_weights(): pl.pallas_call(weights_kernel, out_shape=(full, down, full), in_specs=[AN...  107 us
    pallas_call x1, Pallas kernels, compute_terms(): pl.pallas_call(compute_kernel, out_shape=(jax.ShapeDtypeStruct((count, pa...  26.1 us
    pallas_call x1, Pallas kernels, emit(): pl.pallas_call(emit_kernel, out_shape=(proj, proj, jax.ShapeDtypeStruct(d...  12.4 us

profile of v2, /device:TPU:0, one launch (start us, length us, event | category | flops | bytes accessed | tf_op | source)
XLA Modules:
  0.0 334.7 jit_solution(5620063829797741074)
XLA Ops:
  0.6 0.0 copy-start
  0.6 0.9 dynamic_slice.3
  1.6 0.1 copy.16.gain
  1.7 0.0 copy-start.2
  1.7 2.2 convert_element_type.14.down_src
  3.9 0.0 copy-done
  3.9 0.0 copy-start.1
  3.9 1.3 convert_element_type.15.down_src
  5.2 0.0 copy-done.2
  5.2 1.2 copy-done.1
  6.4 0.3 convert_bitcast_fusion
  6.7 0.3 pad_maximum_fusion.src_one
  7.0 106.9 %gather_weights.1 = (bf16[2,2048,1408]{2,1,0:T(8,128)(2,1)}, bf16[4,1408,512]{2,1,0:T(8,128)(2,1)}, bf16[2,2048,1408]{2,1,0:T(8,128)(2,1)}) custom-call(bf16[2,512,1408]{2,1,0:T(8,128)(2,1)S(1)} %pad_maximum_fusion.src_one, bf16[1408,512]{1,0:T(8,128)(2,1)S(1)} %convert_element_type.14.down_src, f32[512,1408]{1,0:T(8,128)} %gate_two.1, f32[512,1408]{1,0:T(8,128)} %up_two.1, ...), custom_call_target="tpu_custom_call" | custom-call | tf_op jit(solution)/shard_map/gather_weights/pallas_call | solution.py:452
  113.9 26.1 %compute_terms.1 = (bf16[1024,2048]{1,0:T(8,128)(2,1)}, bf16[2048,1408]{1,0:T(8,128)(2,1)}, bf16[2048,1408]{1,0:T(8,128)(2,1)}, bf16[1408,2048]{1,0:T(8,128)(2,1)}) custom-call(bf16[1024,2048]{1,0:T(8,128)(2,1)} %bitcast.8, bf16[2,2048,1408]{2,1,0:T(8,128)(2,1)} %get-tuple-element.20.w, bf16[4,1408,512]{2,1,0:T(8,128)(2,1)} %get-tuple-element.21.down), custom_call_target="tpu_custom_call" | custom-call | flops 17716740096 | bytes 34603008 | tf_op jit(solution)/shard_map/compute_terms/pallas_call | solution.py:569
  140.0 181.3 %sum_norm_blocks.1 = (bf16[256,2048]{1,0:T(8,128)(2,1)}, bf16[2,2048,1408]{2,1,0:T(8,128)(2,1)}, bf16[4,1408,512]{2,1,0:T(8,128)(2,1)}) custom-call(bf16[1024,2048]{1,0:T(8,128)(2,1)} %get-tuple-element.22.terms_one, bf16[1024,2048]{1,0:T(8,128)(2,1)} %bitcast.9, f32[1,2048]{1,0:T(1,128)} %bitcast.11, ...), custom_call_target="tpu_custom_call", output_to_operand_aliasing={{1}: (3, {})} | custom-call | tf_op jit(solution)/shard_map/sum_norm_blocks/pallas_call | solution.py:974
  321.3 0.0 copy-start.3
  321.4 12.4 %emit_projections.1 = (bf16[2048,1408]{1,0:T(8,128)(2,1)}, bf16[2048,1408]{1,0:T(8,128)(2,1)}, bf16[1408,2048]{1,0:T(8,128)(2,1)}) custom-call(bf16[2,2048,1408]{2,1,0:T(8,128)(2,1)} %get-tuple-element.28.w, bf16[4,1408,512]{2,1,0:T(8,128)(2,1)} %get-tuple-element.29.down), custom_call_target="tpu_custom_call" | custom-call | tf_op jit(solution)/shard_map/emit_projections/pallas_call | solution.py:1037
  333.7 0.0 copy-done.3
  333.7 1.0 copy.19
Async XLA Ops:
  0.6 3.3 copy-start
  1.7 3.5 %copy-start.2 = (f32[512,1408]{1,0:T(8,128)S(1)}, f32[512,1408]{1,0:T(8,128)}, u32[]{:S(2)}) copy-start(f32[512,1408]{1,0:T(8,128)} %param.9) | copy-start | bytes 8650756
  3.9 2.5 copy-start.1
  321.3 12.4 %copy-start.3 = (bf16[256,2048]{1,0:T(8,128)(2,1)S(1)}, bf16[256,2048]{1,0:T(8,128)(2,1)}, u32[]{:S(2)}) copy-start(bf16[256,2048]{1,0:T(8,128)(2,1)} %get-tuple-element.24) | copy-start | bytes 3145732
